TPU v7x, 256 devices: a whole 4x4x8 slice. The times are simulated.
256 devices in a mesh: fs: 32 (over z, x), tp: 8 (over y, core).
Axes of the slice: x: 4, y: 4, z: 8, core: 2. Of those that a mesh axis runs over, the one named last changes fastest.
Arguments:
- tokens: bfloat16 [32768, 2048], P(('fs', 'tp')), may hold values from -6 to 6
- gate_pre: bfloat16 [32768, 5632], P('fs', 'tp'), may hold values from -6 to 6
- value_pre: bfloat16 [32768, 5632], P('fs', 'tp'), may hold values from -6 to 6
- up_gate_w: bfloat16 [2048, 5632], P('fs', 'tp'), may hold values from -0.078125 to 0.078125
- up_value_w: bfloat16 [2048, 5632], P('fs', 'tp'), may hold values from -0.078125 to 0.078125
- conv_weight: float32 [3, 5632], P(None, 'tp'), may hold values from -3 to 3
- conv_bias: float32 [5632], P('tp'), may hold values from -3 to 3
- hidden_grad: bfloat16 [32768, 5632], P('fs', 'tp'), may hold values from -6 to 6
Outputs:
- input_grad: bfloat16 [32768, 2048], P(('fs', 'tp'))
- up_gate_grad: float32 [2048, 5632], P('fs', 'tp')
- up_value_grad: float32 [2048, 5632], P('fs', 'tp')
- conv_weight_grad: float32 [3, 5632], P(None, 'tp')
- conv_bias_grad: float32 [5632], P('tp')
All inputs are finite; a program needn't handle non-finite values.
Results may differ from a plain program's by a relative error of at most 0.013.
Values may be sent and summed in bfloat16 or wider, within the bound.
No kernel may reach another device: no remote copies, remote signals or barrier semaphores. Data moves between devices by JAX's collectives and lax.ppermute only.
A program may use at most 128 MiB of HBM per device.

v0:
```python
import jax
import jax.numpy as jnp
from jax import lax
from jax.sharding import Mesh
from jax.sharding import PartitionSpec as P

FS = ("fs_0", "fs_1")
FS_TP = ("fs_0", "fs_1", "tp")


def copy_for_each(shard, axis):
    peers = lax.axis_size(axis)
    return lax.all_to_all(
        jnp.broadcast_to(shard[None], (peers, *shard.shape)), axis, 0, 0, tiled=True
    )


def taken_together(shard, axis):
    return copy_for_each(shard, axis).sum(axis=0)


def in_one_piece(arrays, axis, dim, along):
    ends, at = ([], 0)
    for a in arrays[:-1]:
        at += a.shape[along]
        ends.append(at)
    both = jnp.concatenate(arrays, axis=along)
    return tuple(jnp.split(lax.all_gather(both, axis, axis=dim, tiled=True), ends, axis=along))


def summed_rows(subtotal, axes):
    return lax.psum_scatter(
        subtotal.astype(jnp.bfloat16), axes, scatter_dimension=0, tiled=True
    ).astype(jnp.float32)


def in_blocks(shard, dim, peers):
    lengths = shard.shape
    blocks = shard.reshape(*lengths[:dim], peers, lengths[dim] // peers, *lengths[dim + 1 :])
    return jnp.moveaxis(blocks, dim, 0)


def summed_on_arrival(shard, axis, dim):
    blocks = in_blocks(shard, dim, lax.axis_size(axis))
    arrived = lax.all_to_all(blocks, axis, split_axis=0, concat_axis=0, tiled=True)
    return arrived.astype(jnp.float32).sum(axis=0)


def contract_rows(left, right):
    return lax.dot_general(
        left, right, (((0,), (0,)), ((), ())), preferred_element_type=jnp.float32
    )


def contract_cols(left, right):
    return lax.dot_general(
        left, right, (((1,), (1,)), ((), ())), preferred_element_type=jnp.float32
    )


def on_device(
    tokens, gate_pre, value_pre, up_gate_w, up_value_w, conv_weight, conv_bias, hidden_grad
):
    length = gate_pre.shape[0]
    col_count = gate_pre.shape[1]
    scale = float(length * lax.axis_size(FS)) ** (-0.5)
    gate_float = gate_pre.astype(jnp.float32)
    padded = jnp.pad(gate_float, ((2, 0), (0, 0)))
    gate_conv = (
        conv_bias
        + conv_weight[0] * padded[:length]
        + conv_weight[1] * padded[1 : length + 1]
        + conv_weight[2] * padded[2:]
    )
    active, gelu_back = jax.vjp(jax.nn.gelu, gate_conv)
    grad_float = hidden_grad.astype(jnp.float32)
    value_grad = (grad_float * active).astype(jnp.bfloat16)
    conv_grad = gelu_back(grad_float * value_pre.astype(jnp.float32))[0]
    shifted = jnp.pad(conv_grad, ((0, 2), (0, 0)))
    gate_grad = (
        conv_weight[2] * conv_grad
        + conv_weight[1] * shifted[1 : length + 1]
        + conv_weight[0] * shifted[2:]
    ).astype(jnp.bfloat16)
    conv_terms = jnp.stack(
        [
            jnp.sum(conv_grad * padded[:length], axis=0),
            jnp.sum(conv_grad * padded[1 : length + 1], axis=0),
            jnp.sum(conv_grad * padded[2:], axis=0),
            jnp.sum(conv_grad, axis=0),
        ]
    )
    conv_total = taken_together(conv_terms, FS) * scale
    whole_tokens = lax.all_gather(tokens, "tp", axis=0, tiled=True)
    full_gate, full_value = in_one_piece((up_gate_w, up_value_w), FS, 0, 1)
    joined = summed_rows(
        jnp.concatenate(
            [contract_rows(whole_tokens, gate_grad), contract_rows(whole_tokens, value_grad)],
            axis=1,
        ),
        FS,
    )
    gate_out = joined[:, :col_count] * scale
    value_out = joined[:, col_count:] * scale
    input_grad = summed_on_arrival(
        (contract_cols(gate_grad, full_gate) + contract_cols(value_grad, full_value)).astype(
            jnp.bfloat16
        ),
        "tp",
        0,
    ).astype(jnp.bfloat16)
    return (input_grad, gate_out, value_out, conv_total[:3], conv_total[3])


def solution(mesh):
    finer = Mesh(mesh.devices.reshape(8, 4, mesh.shape["tp"]), ("fs_0", "fs_1", "tp"))
    in_specs = (
        P(FS_TP, None),
        P(FS, "tp"),
        P(FS, "tp"),
        P(FS, "tp"),
        P(FS, "tp"),
        P(None, "tp"),
        P("tp"),
        P(FS, "tp"),
    )
    out_specs = (P(FS_TP, None), P(FS, "tp"), P(FS, "tp"), P(None, "tp"), P("tp"))
    return jax.shard_map(
        on_device, mesh=finer, in_specs=in_specs, out_specs=out_specs, check_vma=False
    )
```

profile of v0, /device:TPU:8, one launch (start us, length us, event | category | flops | bytes accessed | tf_op | source)
XLA Modules:
  0.0 376.6 jit_solution(886776564580868433)
XLA Ops:
  7.2 0.0 copy-start
  7.2 0.0 copy-start.7
  7.2 0.0 copy-start.8
  7.2 0.0 copy-start.2
  7.2 0.0 all-gather.5.cloned.1.call-start
  7.3 0.7 all-gather.5.cloned.1.call-update
  7.9 0.0 all-gather.3.cloned.1.call-start
  8.0 1.8 pad_maximum_fusion.1
  9.8 0.0 all-gather.3.cloned.1.call-update
  9.8 0.0 reduce-scatter.4.cloned.1.call-start
  9.9 0.0 copy-start.3
  9.9 1.8 convert_element_type.30
  11.7 0.0 copy-done.7
  11.8 0.0 copy-done
  11.8 0.0 copy-done.8
  11.8 0.0 copy-done.2
  11.8 0.0 copy-done.3
  11.8 6.5 %multiply_reduce_fusion.2 = (f32[704]{0:T(1024)S(1)}, f32[704]{0:T(1024)S(1)}, f32[704]{0:T(1024)S(1)}, f32[704]{0:T(1024)S(1)}, f32[1024,704]{0,1:T(8,128)S(1)}, /*index=5*/f32[1024,704]{0,1:T(8,128)}) fusion(f32[1024,704]{0,1:T(8,128)S(1)} %convert_element_type.30, bf16[1024,704]{0,1:T(8,128)(2,1)S(1)} %copy-done, bf16[1024,704]{0,1:T(8,128)(2,1)S(1)} %copy-done.2, ...), kind=kLoop, calls=%fused_computation.31 | loop fusion | flops 25949440 | bytes 12998656 | tf_op jit(solution)/shard_map/reduce_sum | solution.py:87
  18.3 3.0 fusion.8
  21.3 25.0 %all-gather.5.cloned.1.call-done = bf16[1024,2048]{1,0:T(8,128)(2,1)} async-done(((bf16[128,2048]{1,0:T(8,128)(2,1)}), bf16[1024,2048]{1,0:T(8,128)(2,1)}) %all-gather.5.cloned.1.call-update) | async-done | bytes 4194320 | tf_op jit(solution)/shard_map/all_gather | solution.py:94
  46.4 5.9 %fusion.3 = bf16[2048,704]{0,1:T(8,128)(2,1)S(1)} fusion(bf16[1024,704]{0,1:T(8,128)(2,1)} %fusion.8, bf16[1024,2048]{1,0:T(8,128)(2,1)} %all-gather.5.cloned.1.call-done), kind=kOutput, calls=%fused_computation.15 | convolution fusion | flops 2954231808 | bytes 8519680 | tf_op jit(solution)/shard_map/dot_general | solution.py:50
  52.3 0.0 copy-done.1
  52.3 0.0 copy-done.4
  52.3 0.0 copy-done.10
  52.3 3.9 %fusion.4 = bf16[2048,704]{0,1:T(8,128)(2,1)S(1)} fusion(bf16[1024,2048]{1,0:T(8,128)(2,1)S(1)} %copy-done.10, bf16[1024,704]{0,1:T(8,128)(2,1)S(1)} %copy-done.4, f32[1024,704]{0,1:T(8,128)S(1)} %copy-done.1), kind=kOutput, calls=%fused_computation.16 | convolution fusion | flops 2962161664 | bytes 11403264 | tf_op jit(solution)/shard_map/dot_general | solution.py:50
  56.2 3.1 pad_maximum_fusion
  59.4 8.4 %copy.22 = bf16[2048,1408]{1,0:T(8,128)(2,1)} copy(bf16[2048,1408]{0,1:T(8,128)(2,1)} %pad_maximum_fusion) | data formatting | bytes 11534336
  67.8 0.0 reduce-scatter.4.cloned.1.call-update
  67.8 0.8 broadcast_in_dim.2
  68.6 10.0 %all-to-all-start.1 = ((f32[32,4,704]{2,1,0:T(4,128)}), f32[32,4,704]{2,1,0:T(4,128)S(1)}, u32[]{:S(2)}, u32[]{:S(2)}) async-start(f32[32,4,704]{2,1,0:T(4,128)} %broadcast_in_dim.2), calls=%async_computation.1 | async-start | bytes 786432 | tf_op jit(solution)/shard_map/all_to_all | solution.py:13
  78.7 60.2 %all-gather.3.cloned.1.call-done = bf16[2048,1408]{1,0:T(8,128)(2,1)} async-done(((bf16[64,1408]{1,0:T(8,128)(2,1)}), bf16[2048,1408]{1,0:T(8,128)(2,1)}) %all-gather.3.cloned.1.call-update) | async-done | bytes 5767184 | tf_op jit(solution)/shard_map/all_gather | solution.py:28
  138.9 6.0 %fusion.1 = f32[1024,2048]{1,0:T(8,128)S(1)} fusion(bf16[1024,704]{0,1:T(8,128)(2,1)} %fusion.8, bf16[2048,1408]{1,0:T(8,128)(2,1)} %all-gather.3.cloned.1.call-done), kind=kOutput, calls=%fused_computation.13 | convolution fusion | flops 2952790016 | bytes 12976128 | tf_op jit(solution)/shard_map/dot_general | solution.py:56
  144.9 0.0 copy-done.5
  144.9 0.0 copy-done.9
  144.9 7.6 %add_convert_fusion = bf16[1024,2048]{1,0:T(8,128)(2,1)} fusion(f32[1024,2048]{1,0:T(8,128)S(1)} %fusion.1, bf16[2048,1408]{1,0:T(8,128)(2,1)S(1)} %copy-done.9, bf16[1024,704]{0,1:T(8,128)(2,1)S(1)} %copy-done.5, f32[1024,704]{0,1:T(8,128)S(1)} %copy-done.1), kind=kOutput, calls=%fused_computation | convolution fusion | flops 2964914176 | bytes 20054016 | tf_op jit(solution)/shard_map/dot_general | solution.py:56
  152.5 0.0 all-to-all-done.1
  152.5 5.0 %all-to-all-start = ((bf16[8,128,2048]{2,1,0:T(8,128)(2,1)}), bf16[8,128,2048]{2,1,0:T(8,128)(2,1)}, u32[]{:S(2)}, u32[]{:S(2)}) async-start(bf16[8,128,2048]{2,1,0:T(8,128)(2,1)} %bitcast.11), calls=%async_computation | async-start | bytes 8388608 | tf_op jit(solution)/shard_map/all_to_all | solution.py:45
  157.4 0.1 reduce_sum.62
  157.5 0.0 copy-start.6
  157.5 0.6 slice_reduce_fusion
  158.1 47.6 %all-to-all-done = bf16[8,128,2048]{2,1,0:T(8,128)(2,1)} async-done(((bf16[8,128,2048]{2,1,0:T(8,128)(2,1)}), bf16[8,128,2048]{2,1,0:T(8,128)(2,1)}, u32[]{:S(2)}, u32[]{:S(2)}) %all-to-all-start) | async-done | bytes 4194336 | tf_op jit(solution)/shard_map/all_to_all | solution.py:45
  205.8 4.0 %reduce_sum.57 = bf16[128,2048]{1,0:T(8,128)(2,1)} reduce(bf16[8,128,2048]{2,1,0:T(8,128)(2,1)} %all-to-all-done, bf16[]{:T(256)} %constant.19.clone.1), dimensions={0}, to_apply=%region_0.1 | reduce | flops 1835008 | bytes 4718594 | tf_op jit(solution)/shard_map/reduce_sum | solution.py:46
  209.7 157.4 %reduce-scatter.4.cloned.1.call-done = bf16[64,1408]{1,0:T(8,128)(2,1)} async-done(((bf16[2048,1408]{1,0:T(8,128)(2,1)}), bf16[64,1408]{1,0:T(8,128)(2,1)}) %reduce-scatter.4.cloned.1.call-update) | async-done | bytes 180240
  367.2 1.1 copy.23
  368.4 0.0 copy-done.6
  368.4 0.1 slice_multiply_fusion
  368.4 0.8 copy.21
  369.3 0.8 copy.20
  (13 shorter events, 0.1 us)
Async XLA Ops:
  7.2 4.6 %copy-start = (bf16[1024,704]{0,1:T(8,128)(2,1)S(1)}, bf16[1024,704]{0,1:T(8,128)(2,1)}, u32[]{:S(2)}) copy-start(bf16[1024,704]{0,1:T(8,128)(2,1)} %param.9) | copy-start | bytes 4325380
  7.2 4.5 %copy-start.7 = (f32[3,704]{1,0:T(4,128)S(1)}, f32[3,704]{1,0:T(4,128)}, u32[]{:S(2)}) copy-start(f32[3,704]{1,0:T(4,128)} %param.13) | copy-start | bytes 25348
  7.2 4.6 %copy-start.8 = (f32[704]{0:T(1024)S(1)}, f32[704]{0:T(1024)}, u32[]{:S(2)}) copy-start(f32[704]{0:T(1024)} %param.14) | copy-start | bytes 8452
  7.2 4.6 %copy-start.2 = (bf16[1024,704]{0,1:T(8,128)(2,1)S(1)}, bf16[1024,704]{0,1:T(8,128)(2,1)}, u32[]{:S(2)}) copy-start(bf16[1024,704]{0,1:T(8,128)(2,1)} %param.10) | copy-start | bytes 4325380
  7.2 39.2 %all-gather.5.cloned.1.call-start = ((), (), s32[]{:S(2)}) async-start(), calls=%async_computation.4 | async-start | bytes 4718592 | tf_op jit(solution)/shard_map/all_gather | solution.py:94
  7.9 131.0 %all-gather.3.cloned.1.call-start = ((), (), s32[]{:S(2)}) async-start(), calls=%async_computation.3 | async-start | bytes 5947392 | tf_op jit(solution)/shard_map/all_gather | solution.py:28
  9.8 357.4 %reduce-scatter.4.cloned.1.call-start = ((), (), s32[]{:S(2)}) async-start(), calls=%async_computation.5 | async-start | bytes 5947392
  9.9 1.9 copy-start.3
  21.3 31.0 %copy-start.1 = (f32[1024,704]{0,1:T(8,128)S(1)}, f32[1024,704]{0,1:T(8,128)}, u32[]{:S(2)}) copy-start(f32[1024,704]{0,1:T(8,128)} %get-tuple-element.33) | copy-start | bytes 8650756
  46.4 5.9 %copy-start.4 = (bf16[1024,704]{0,1:T(8,128)(2,1)S(1)}, bf16[1024,704]{0,1:T(8,128)(2,1)}, u32[]{:S(2)}) copy-start(bf16[1024,704]{0,1:T(8,128)(2,1)} %param.15) | copy-start | bytes 4325380
  46.4 5.9 %copy-start.10 = (bf16[1024,2048]{1,0:T(8,128)(2,1)S(1)}, bf16[1024,2048]{1,0:T(8,128)(2,1)}, u32[]{:S(2)}) copy-start(bf16[1024,2048]{1,0:T(8,128)(2,1)} %all-gather.5.cloned.1.call-done) | copy-start | bytes 12582916
  68.6 83.8 %all-to-all-start.1 = ((f32[32,4,704]{2,1,0:T(4,128)}), f32[32,4,704]{2,1,0:T(4,128)S(1)}, u32[]{:S(2)}, u32[]{:S(2)}) async-start(f32[32,4,704]{2,1,0:T(4,128)} %broadcast_in_dim.2), calls=%async_computation.1 | async-start | bytes 786432 | tf_op jit(solution)/shard_map/all_to_all | solution.py:13
  138.9 6.0 %copy-start.5 = (bf16[1024,704]{0,1:T(8,128)(2,1)S(1)}, bf16[1024,704]{0,1:T(8,128)(2,1)}, u32[]{:S(2)}) copy-start(bf16[1024,704]{0,1:T(8,128)(2,1)} %param.15) | copy-start | bytes 4325380
  138.9 6.0 %copy-start.9 = (bf16[2048,1408]{1,0:T(8,128)(2,1)S(1)}, bf16[2048,1408]{1,0:T(8,128)(2,1)}, u32[]{:S(2)}) copy-start(bf16[2048,1408]{1,0:T(8,128)(2,1)} %all-gather.3.cloned.1.call-done) | copy-start | bytes 17301508
  152.5 53.3 %all-to-all-start = ((bf16[8,128,2048]{2,1,0:T(8,128)(2,1)}), bf16[8,128,2048]{2,1,0:T(8,128)(2,1)}, u32[]{:S(2)}, u32[]{:S(2)}) async-start(bf16[8,128,2048]{2,1,0:T(8,128)(2,1)} %bitcast.11), calls=%async_computation | async-start | bytes 8388608 | tf_op jit(solution)/shard_map/all_to_all | solution.py:45
  157.5 210.8 %copy-start.6 = (f32[4,704]{1,0:T(4,128)}, f32[4,704]{1,0:T(4,128)S(1)}, u32[]{:S(2)}) copy-start(f32[4,704]{1,0:T(4,128)S(1)} %broadcast_multiply_fusion) | copy-start | bytes 33796
Sparse Core Ops, SparseCore 0:
  9.9 36.4 all-gather.4
  49.5 89.3 all-gather.2
  142.9 224.2 reduce-scatter.3
where the time goes:
time: 377 us
  waiting for transfers between devices  291 us (77%)
  matrix products  23.3 us (6%)
  other arithmetic  20.5 us (5%)
  starting transfers between devices  15.1 us (4%)
  between operations  14 us (4%)
  local copies, waits for them, and re-layouts  12.7 us (3%)
    unnamed x4, waiting for transfers between devices  158 us
    all_gather x1, waiting for transfers between devices, in_one_piece(): lax.all_gather(both, axis, axis=dim, tiled=True)  60.2 us
    all_to_all x1, waiting for transfers between devices, summed_on_arrival(): lax.all_to_all(blocks, axis, split_axis=0, concat_axis=0, tiled=True)  47.6 us
    all_gather x1, waiting for transfers between devices, on_device(): whole_tokens = lax.all_gather(tokens, 'tp', axis=0, tiled=True)  25 us
    dot_general x2, matrix products, contract_cols(): lax.dot_general(left, right, (((1,), (1,)), ((), ())), preferred_element_...  13.5 us
    unnamed x26, local copies, waits for them, and re-layouts  11.2 us
    all_to_all x1, starting transfers between devices, copy_for_each(): lax.all_to_all(jnp.broadcast_to(shard[None], (peers, *shard.shape)), axis...  10 us
    dot_general x2, matrix products, contract_rows(): lax.dot_general(left, right, (((0,), (0,)), ((), ())), preferred_element_...  9.78 us
  transfers between devices with their start and end apart: 5, of which 4 were waited for; matrix products, arithmetic and copies ran while one was open for 14% of the time, Pallas kernels for 0%

commit v1 on v0

--- a/solution.py
+++ b/solution.py
@@ -6,6 +6,17 @@
 
 FS = ("fs_0", "fs_1")
 FS_TP = ("fs_0", "fs_1", "tp")
+
+
+def around_the_ring(x, axis, along):
+    size = lax.axis_size(axis)
+    forward = [(i, (i + 1) % size) for i in range(size)]
+    parts = [x]
+    for reach in range(1, size):
+        parts = [lax.ppermute(parts[0], axis, forward), *parts]
+    whole = jnp.concatenate(parts, axis=along)
+    shift = (lax.axis_index(axis) + 1) * parts[-1].shape[along]
+    return jnp.roll(whole, shift, axis=along)
 
 
 def copy_for_each(shard, axis):
@@ -91,7 +102,7 @@
         ]
     )
     conv_total = taken_together(conv_terms, FS) * scale
-    whole_tokens = lax.all_gather(tokens, "tp", axis=0, tiled=True)
+    whole_tokens = around_the_ring(tokens, "tp", 0)
     full_gate, full_value = in_one_piece((up_gate_w, up_value_w), FS, 0, 1)
     joined = summed_rows(
         jnp.concatenate(

time: 377 us -> 343 us (0.910)
  waiting for transfers between devices: 291 us -> 246 us
  starting transfers between devices: 15.1 us -> 23.2 us
  local copies, waits for them, and re-layouts: 12.7 us -> 18.3 us
    all_gather x1, waiting for transfers between devices: 60.2 us -> 0.02 us  [in_one_piece(): lax.all_gather(both, axis, axis=dim, tiled=True)]
    ppermute x0 -> x7, waiting for transfers between devices: none -> 50.1 us  [around_the_ring(): parts = [lax.ppermute(parts[0], axis, forward), *parts]]
    all_gather x1 -> x0, waiting for transfers between devices: 25 us -> none  [on_device(): whole_tokens = lax.all_gather(tokens, 'tp', axis=0, tiled=True)]
    unnamed x4 -> x3, waiting for transfers between devices: 158 us -> 146 us
    all_to_all x1, starting transfers between devices: 4.97 us -> 11.6 us  [summed_on_arrival(): lax.all_to_all(blocks, axis, split_axis=0, concat_axis=0, tiled=True)]
    unnamed x26 -> x59, local copies, waits for them, and re-layouts: 11.2 us -> 16.8 us
  transfers between devices with their start and end apart: 5 -> 11, of which waited for: 4 -> 10; matrix products, arithmetic and copies ran while one was open for 14% -> 16% of each run, Pallas kernels for 0% -> 0%
where the time goes in v1:
time: 343 us
  waiting for transfers between devices  246 us (72%)
  starting transfers between devices  23.2 us (7%)
  matrix products  21.3 us (6%)
  other arithmetic  19.5 us (6%)
  local copies, waits for them, and re-layouts  18.3 us (5%)
  between operations  14.5 us (4%)
    unnamed x3, waiting for transfers between devices  146 us
    ppermute x7, waiting for transfers between devices, around_the_ring(): parts = [lax.ppermute(parts[0], axis, forward), *parts]  50.1 us
    all_to_all x1, waiting for transfers between devices, summed_on_arrival(): lax.all_to_all(blocks, axis, split_axis=0, concat_axis=0, tiled=True)  47.6 us
    unnamed x59, local copies, waits for them, and re-layouts  16.8 us
    dot_general x2, matrix products, contract_cols(): lax.dot_general(left, right, (((1,), (1,)), ((), ())), preferred_element_...  13.6 us
    all_to_all x1, starting transfers between devices, summed_on_arrival(): lax.all_to_all(blocks, axis, split_axis=0, concat_axis=0, tiled=True)  11.6 us
    all_to_all x1, starting transfers between devices, copy_for_each(): lax.all_to_all(jnp.broadcast_to(shard[None], (peers, *shard.shape)), axis...  11.5 us
    dot_general x2, matrix products, contract_rows(): lax.dot_general(left, right, (((0,), (0,)), ((), ())), preferred_element_...  7.73 us
  transfers between devices with their start and end apart: 11, of which 10 were waited for; matrix products, arithmetic and copies ran while one was open for 16% of the time, Pallas kernels for 0%

profile of v1, /device:TPU:8, one launch (start us, length us, event | category | flops | bytes accessed | tf_op | source)
XLA Modules:
  0.0 342.7 jit_solution(10365677605329927463)
XLA Ops:
  7.2 0.0 all-gather.2.cloned.1.call-start
  7.2 1.7 pad_maximum_fusion.1
  8.9 0.0 all-gather.2.cloned.1.call-update
  9.0 0.0 reduce-scatter.4.cloned.1.call-start
  9.0 0.0 copy-start
  9.0 0.0 copy-start.11
  9.0 0.0 copy-start.12
  9.1 0.0 collective-permute-start
  9.1 8.8 %collective-permute-done = bf16[128,2048]{1,0:T(8,128)(2,1)S(1)} collective-permute-done((bf16[128,2048]{1,0:T(8,128)(2,1)}, bf16[128,2048]{1,0:T(8,128)(2,1)S(1)}, u32[]{:S(2)}, u32[]{:S(2)}) %collective-permute-start) | collective-permute-done | bytes 524320 | tf_op jit(solution)/shard_map/ppermute | solution.py:16
  17.9 8.6 %collective-permute-done.1 = bf16[128,2048]{1,0:T(8,128)(2,1)S(1)} collective-permute-done((bf16[128,2048]{1,0:T(8,128)(2,1)S(1)}, bf16[128,2048]{1,0:T(8,128)(2,1)S(1)}, u32[]{:S(2)}, u32[]{:S(2)}) %collective-permute-start.1) | collective-permute-done | bytes 524320 | tf_op jit(solution)/shard_map/ppermute | solution.py:16
  26.5 8.6 %collective-permute-done.2 = bf16[128,2048]{1,0:T(8,128)(2,1)S(1)} collective-permute-done((bf16[128,2048]{1,0:T(8,128)(2,1)S(1)}, bf16[128,2048]{1,0:T(8,128)(2,1)S(1)}, u32[]{:S(2)}, u32[]{:S(2)}) %collective-permute-start.2) | collective-permute-done | bytes 524320 | tf_op jit(solution)/shard_map/ppermute | solution.py:16
  35.1 8.6 %collective-permute-done.3 = bf16[128,2048]{1,0:T(8,128)(2,1)S(1)} collective-permute-done((bf16[128,2048]{1,0:T(8,128)(2,1)S(1)}, bf16[128,2048]{1,0:T(8,128)(2,1)S(1)}, u32[]{:S(2)}, u32[]{:S(2)}) %collective-permute-start.3) | collective-permute-done | bytes 524320 | tf_op jit(solution)/shard_map/ppermute | solution.py:16
  43.7 8.6 %collective-permute-done.4 = bf16[128,2048]{1,0:T(8,128)(2,1)S(1)} collective-permute-done((bf16[128,2048]{1,0:T(8,128)(2,1)S(1)}, bf16[128,2048]{1,0:T(8,128)(2,1)S(1)}, u32[]{:S(2)}, u32[]{:S(2)}) %collective-permute-start.4) | collective-permute-done | bytes 524320 | tf_op jit(solution)/shard_map/ppermute | solution.py:16
  52.3 0.0 copy-start.9
  52.3 0.0 collective-permute-start.5
  52.4 1.9 convert_element_type.30
  54.3 6.7 %collective-permute-done.5 = bf16[128,2048]{1,0:T(8,128)(2,1)} collective-permute-done((bf16[128,2048]{1,0:T(8,128)(2,1)S(1)}, bf16[128,2048]{1,0:T(8,128)(2,1)}, u32[]{:S(2)}, u32[]{:S(2)}) %collective-permute-start.5) | collective-permute-done | bytes 524320 | tf_op jit(solution)/shard_map/ppermute | solution.py:16
  61.1 6.6 %multiply_reduce_fusion.2 = (f32[704]{0:T(1024)S(1)}, f32[704]{0:T(1024)S(1)}, f32[704]{0:T(1024)S(1)}, f32[704]{0:T(1024)S(1)}, f32[1024,704]{0,1:T(8,128)S(1)}, /*index=5*/f32[1024,704]{0,1:T(8,128)}) fusion(f32[1024,704]{0,1:T(8,128)S(1)} %convert_element_type.30, bf16[1024,704]{0,1:T(8,128)(2,1)S(1)} %copy-done, bf16[1024,704]{0,1:T(8,128)(2,1)S(1)} %copy-done.11, ...), kind=kLoop, calls=%fused_computation.33 | loop fusion | flops 25949440 | bytes 12998656 | tf_op jit(solution)/shard_map/reduce_sum | solution.py:98
  67.7 2.1 fusion.16
  69.8 0.2 collective-permute-done.6
  70.0 1.7 constant_dynamic-update-slice_fusion.15
  71.7 0.0 copy-start.2
  71.7 1.2 constant_dynamic-update-slice_fusion.14
  73.2 1.1 constant_dynamic-update-slice_fusion.7
  74.3 1.1 constant_dynamic-update-slice_fusion.6
  75.7 0.0 copy-start.13
  75.7 3.4 fusion.7
  79.1 4.3 %fusion.4 = bf16[2048,704]{0,1:T(8,128)(2,1)S(1)} fusion(bf16[2048,2048]{1,0:T(8,128)(2,1)S(1)} %constant_dynamic-update-slice_fusion, s32[]{:T(128)S(6)} %select_n.14, bf16[1024,704]{0,1:T(8,128)(2,1)S(1)} %copy-done.13, f32[1024,704]{0,1:T(8,128)S(1)} %copy-done.1), kind=kOutput, calls=%fused_computation.10 | convolution fusion | flops 2962161664 | bytes 11403268 | tf_op jit(solution)/shard_map/dot_general | solution.py:61
  83.4 3.2 pad_maximum_fusion
  86.6 8.4 %copy.22 = bf16[2048,1408]{1,0:T(8,128)(2,1)} copy(bf16[2048,1408]{0,1:T(8,128)(2,1)} %pad_maximum_fusion) | data formatting | bytes 11534336
  95.0 0.0 reduce-scatter.4.cloned.1.call-update
  95.1 0.8 broadcast_in_dim.2
  95.9 11.5 %all-to-all-start.1 = ((f32[32,4,704]{2,1,0:T(4,128)}), f32[32,4,704]{2,1,0:T(4,128)S(1)}, u32[]{:S(2)}, u32[]{:S(2)}) async-start(f32[32,4,704]{2,1,0:T(4,128)} %broadcast_in_dim.2), calls=%async_computation.1 | async-start | bytes 786432 | tf_op jit(solution)/shard_map/all_to_all | solution.py:24
  107.4 0.0 all-gather.2.cloned.1.call-done
  107.5 0.0 copy-start.14
  107.5 6.0 %fusion.11 = f32[1024,2048]{1,0:T(8,128)S(1)} fusion(bf16[1024,704]{0,1:T(8,128)(2,1)} %copy-done.15, bf16[2048,1408]{1,0:T(8,128)(2,1)} %all-gather.2.cloned.1.call-done), kind=kOutput, calls=%fused_computation.17 | convolution fusion | flops 2952790016 | bytes 12976128 | tf_op jit(solution)/shard_map/dot_general | solution.py:67
  113.5 7.6 %add_convert_fusion = bf16[1024,2048]{1,0:T(8,128)(2,1)} fusion(f32[1024,2048]{1,0:T(8,128)S(1)} %fusion.11, bf16[2048,1408]{1,0:T(8,128)(2,1)S(1)} %copy-done.19, bf16[1024,704]{0,1:T(8,128)(2,1)S(1)} %copy-done.14, f32[1024,704]{0,1:T(8,128)S(1)} %copy-done.1), kind=kOutput, calls=%fused_computation | convolution fusion | flops 2964914176 | bytes 20054016 | tf_op jit(solution)/shard_map/dot_general | solution.py:67
  121.0 2.2 all-to-all-done.1
  123.3 11.6 %all-to-all-start = ((bf16[8,128,2048]{2,1,0:T(8,128)(2,1)}), bf16[8,128,2048]{2,1,0:T(8,128)(2,1)}, u32[]{:S(2)}, u32[]{:S(2)}) async-start(bf16[8,128,2048]{2,1,0:T(8,128)(2,1)} %bitcast.5), calls=%async_computation | async-start | bytes 8388608 | tf_op jit(solution)/shard_map/all_to_all | solution.py:56
  134.9 0.1 reduce_sum.62
  135.0 0.6 slice_reduce_fusion
  135.6 47.6 %all-to-all-done = bf16[8,128,2048]{2,1,0:T(8,128)(2,1)} async-done(((bf16[8,128,2048]{2,1,0:T(8,128)(2,1)}), bf16[8,128,2048]{2,1,0:T(8,128)(2,1)}, u32[]{:S(2)}, u32[]{:S(2)}) %all-to-all-start) | async-done | bytes 4194336 | tf_op jit(solution)/shard_map/all_to_all | solution.py:56
  183.2 3.9 %reduce_sum.57 = bf16[128,2048]{1,0:T(8,128)(2,1)} reduce(bf16[8,128,2048]{2,1,0:T(8,128)(2,1)} %all-to-all-done, bf16[]{:T(256)} %constant.42.clone.1), dimensions={0}, to_apply=%region_0.1 | reduce | flops 1835008 | bytes 4718594 | tf_op jit(solution)/shard_map/reduce_sum | solution.py:57
  187.1 145.9 %reduce-scatter.4.cloned.1.call-done = bf16[64,1408]{1,0:T(8,128)(2,1)} async-done(((bf16[2048,1408]{1,0:T(8,128)(2,1)}), bf16[64,1408]{1,0:T(8,128)(2,1)}) %reduce-scatter.4.cloned.1.call-update) | async-done | bytes 180240
  333.0 1.1 copy.23
  334.2 0.1 slice_multiply_fusion
  334.2 0.8 copy.20
  335.1 0.8 copy.21
  (58 shorter events, 0.7 us)
Async XLA Ops:
  7.2 47.1 %copy-start.17 = (f32[3,704]{1,0:T(4,128)S(1)}, f32[3,704]{1,0:T(4,128)}, u32[]{:S(2)}) copy-start(f32[3,704]{1,0:T(4,128)} %param.13) | copy-start | bytes 25348
  7.2 53.9 %copy-start.18 = (f32[704]{0:T(1024)S(1)}, f32[704]{0:T(1024)}, u32[]{:S(2)}) copy-start(f32[704]{0:T(1024)} %param.14) | copy-start | bytes 8452
  7.2 100.3 %all-gather.2.cloned.1.call-start = ((), (), s32[]{:S(2)}) async-start(), calls=%async_computation.3 | async-start | bytes 5947392 | tf_op jit(solution)/shard_map/all_gather | solution.py:39
  9.0 324.0 %reduce-scatter.4.cloned.1.call-start = ((), (), s32[]{:S(2)}) async-start(), calls=%async_computation.4 | async-start | bytes 5947392
  9.0 52.1 %copy-start = (bf16[1024,704]{0,1:T(8,128)(2,1)S(1)}, bf16[1024,704]{0,1:T(8,128)(2,1)}, u32[]{:S(2)}) copy-start(bf16[1024,704]{0,1:T(8,128)(2,1)} %param.9) | copy-start | bytes 4325380
  9.0 52.1 %copy-start.11 = (bf16[1024,704]{0,1:T(8,128)(2,1)S(1)}, bf16[1024,704]{0,1:T(8,128)(2,1)}, u32[]{:S(2)}) copy-start(bf16[1024,704]{0,1:T(8,128)(2,1)} %param.10) | copy-start | bytes 4325380
  9.0 52.1 %copy-start.12 = (bf16[1024,704]{0,1:T(8,128)(2,1)S(1)}, bf16[1024,704]{0,1:T(8,128)(2,1)}, u32[]{:S(2)}) copy-start(bf16[1024,704]{0,1:T(8,128)(2,1)} %param.15) | copy-start | bytes 4325380
  9.1 8.8 %collective-permute-start = (bf16[128,2048]{1,0:T(8,128)(2,1)}, bf16[128,2048]{1,0:T(8,128)(2,1)S(1)}, u32[]{:S(2)}, u32[]{:S(2)}) collective-permute-start(bf16[128,2048]{1,0:T(8,128)(2,1)} %param.8), channel_id=1, source_target_pairs={{0,1},{1,2},{2,3},{3,4},{4,5},{5,6},{6,7},{7,0},{8,9},{9,10},{10,1... | collective-permute-start | bytes 1572872 | tf_op jit(solution)/shard_map/ppermute | solution.py:16
  17.9 8.6 %collective-permute-start.1 = (bf16[128,2048]{1,0:T(8,128)(2,1)S(1)}, bf16[128,2048]{1,0:T(8,128)(2,1)S(1)}, u32[]{:S(2)}, u32[]{:S(2)}) collective-permute-start(bf16[128,2048]{1,0:T(8,128)(2,1)S(1)} %collective-permute-done), channel_id=1, source_target_pairs={{0,1},{1,2},{2,3},{3,4},{4,5},{5,6},{6,7},{7,0},{8,9},{9,10},{10,1... | collective-permute-start | bytes 1572872 | tf_op jit(solution)/shard_map/ppermute | solution.py:16
  26.5 25.8 %copy-start.3 = (bf16[128,2048]{1,0:T(8,128)(2,1)}, bf16[128,2048]{1,0:T(8,128)(2,1)S(1)}, u32[]{:S(2)}) copy-start(bf16[128,2048]{1,0:T(8,128)(2,1)S(1)} %collective-permute-done.1) | copy-start | bytes 1572868
  26.5 8.6 %collective-permute-start.2 = (bf16[128,2048]{1,0:T(8,128)(2,1)S(1)}, bf16[128,2048]{1,0:T(8,128)(2,1)S(1)}, u32[]{:S(2)}, u32[]{:S(2)}) collective-permute-start(bf16[128,2048]{1,0:T(8,128)(2,1)S(1)} %collective-permute-done.1), channel_id=1, source_target_pairs={{0,1},{1,2},{2,3},{3,4},{4,5},{5,6},{6,7},{7,0},{8,9},{9,10},{10,1... | collective-permute-start | bytes 1572872 | tf_op jit(solution)/shard_map/ppermute | solution.py:16
  35.1 17.2 %copy-start.5 = (bf16[128,2048]{1,0:T(8,128)(2,1)}, bf16[128,2048]{1,0:T(8,128)(2,1)S(1)}, u32[]{:S(2)}) copy-start(bf16[128,2048]{1,0:T(8,128)(2,1)S(1)} %collective-permute-done.2) | copy-start | bytes 1572868
  35.1 8.6 %collective-permute-start.3 = (bf16[128,2048]{1,0:T(8,128)(2,1)S(1)}, bf16[128,2048]{1,0:T(8,128)(2,1)S(1)}, u32[]{:S(2)}, u32[]{:S(2)}) collective-permute-start(bf16[128,2048]{1,0:T(8,128)(2,1)S(1)} %collective-permute-done.2), channel_id=1, source_target_pairs={{0,1},{1,2},{2,3},{3,4},{4,5},{5,6},{6,7},{7,0},{8,9},{9,10},{10,1... | collective-permute-start | bytes 1572872 | tf_op jit(solution)/shard_map/ppermute | solution.py:16
  43.7 8.6 %copy-start.7 = (bf16[128,2048]{1,0:T(8,128)(2,1)}, bf16[128,2048]{1,0:T(8,128)(2,1)S(1)}, u32[]{:S(2)}) copy-start(bf16[128,2048]{1,0:T(8,128)(2,1)S(1)} %collective-permute-done.3) | copy-start | bytes 1572868
  43.7 8.6 %collective-permute-start.4 = (bf16[128,2048]{1,0:T(8,128)(2,1)S(1)}, bf16[128,2048]{1,0:T(8,128)(2,1)S(1)}, u32[]{:S(2)}, u32[]{:S(2)}) collective-permute-start(bf16[128,2048]{1,0:T(8,128)(2,1)S(1)} %collective-permute-done.3), channel_id=1, source_target_pairs={{0,1},{1,2},{2,3},{3,4},{4,5},{5,6},{6,7},{7,0},{8,9},{9,10},{10,1... | collective-permute-start | bytes 1572872 | tf_op jit(solution)/shard_map/ppermute | solution.py:16
  52.3 8.7 %copy-start.9 = (bf16[128,2048]{1,0:T(8,128)(2,1)}, bf16[128,2048]{1,0:T(8,128)(2,1)S(1)}, u32[]{:S(2)}) copy-start(bf16[128,2048]{1,0:T(8,128)(2,1)S(1)} %collective-permute-done.4) | copy-start | bytes 1572868
  52.3 8.7 %collective-permute-start.5 = (bf16[128,2048]{1,0:T(8,128)(2,1)S(1)}, bf16[128,2048]{1,0:T(8,128)(2,1)}, u32[]{:S(2)}, u32[]{:S(2)}) collective-permute-start(bf16[128,2048]{1,0:T(8,128)(2,1)S(1)} %collective-permute-done.4), channel_id=1, source_target_pairs={{0,1},{1,2},{2,3},{3,4},{4,5},{5,6},{6,7},{7,0},{8,9},{9,10},{10,1... | collective-permute-start | bytes 1572872 | tf_op jit(solution)/shard_map/ppermute | solution.py:16
  61.1 8.9 %collective-permute-start.6 = (bf16[128,2048]{1,0:T(8,128)(2,1)}, bf16[128,2048]{1,0:T(8,128)(2,1)}, u32[]{:S(2)}, u32[]{:S(2)}) collective-permute-start(bf16[128,2048]{1,0:T(8,128)(2,1)} %collective-permute-done.5), channel_id=1, source_target_pairs={{0,1},{1,2},{2,3},{3,4},{4,5},{5,6},{6,7},{7,0},{8,9},{9,10},{10,1... | collective-permute-start | bytes 1572872 | tf_op jit(solution)/shard_map/ppermute | solution.py:16
  67.7 5.1 %copy-start.10 = (bf16[128,2048]{1,0:T(8,128)(2,1)S(1)}, bf16[128,2048]{1,0:T(8,128)(2,1)}, u32[]{:S(2)}) copy-start(bf16[128,2048]{1,0:T(8,128)(2,1)} %copy-done.9) | copy-start | bytes 1572868
  67.7 5.2 %copy-start.8 = (bf16[128,2048]{1,0:T(8,128)(2,1)S(1)}, bf16[128,2048]{1,0:T(8,128)(2,1)}, u32[]{:S(2)}) copy-start(bf16[128,2048]{1,0:T(8,128)(2,1)} %copy-done.7) | copy-start | bytes 1572868
  69.8 5.8 %copy-start.15 = (bf16[1024,704]{0,1:T(8,128)(2,1)}, bf16[1024,704]{0,1:T(8,128)(2,1)S(1)}, u32[]{:S(2)}) copy-start(bf16[1024,704]{0,1:T(8,128)(2,1)S(1)} %fusion.16) | copy-start | bytes 4325380
  69.8 3.2 copy-start.6
  69.8 3.2 copy-start.4
  71.7 1.4 copy-start.2
  75.6 3.5 %copy-start.1 = (f32[1024,704]{0,1:T(8,128)S(1)}, f32[1024,704]{0,1:T(8,128)}, u32[]{:S(2)}) copy-start(f32[1024,704]{0,1:T(8,128)} %get-tuple-element.33) | copy-start | bytes 8650756
  75.7 3.5 %copy-start.13 = (bf16[1024,704]{0,1:T(8,128)(2,1)S(1)}, bf16[1024,704]{0,1:T(8,128)(2,1)}, u32[]{:S(2)}) copy-start(bf16[1024,704]{0,1:T(8,128)(2,1)} %param.15) | copy-start | bytes 4325380
  95.9 27.3 %all-to-all-start.1 = ((f32[32,4,704]{2,1,0:T(4,128)}), f32[32,4,704]{2,1,0:T(4,128)S(1)}, u32[]{:S(2)}, u32[]{:S(2)}) async-start(f32[32,4,704]{2,1,0:T(4,128)} %broadcast_in_dim.2), calls=%async_computation.1 | async-start | bytes 786432 | tf_op jit(solution)/shard_map/all_to_all | solution.py:24
  107.5 6.0 %copy-start.14 = (bf16[1024,704]{0,1:T(8,128)(2,1)S(1)}, bf16[1024,704]{0,1:T(8,128)(2,1)}, u32[]{:S(2)}) copy-start(bf16[1024,704]{0,1:T(8,128)(2,1)} %param.15) | copy-start | bytes 4325380
  107.5 6.0 %copy-start.19 = (bf16[2048,1408]{1,0:T(8,128)(2,1)S(1)}, bf16[2048,1408]{1,0:T(8,128)(2,1)}, u32[]{:S(2)}) copy-start(bf16[2048,1408]{1,0:T(8,128)(2,1)} %all-gather.2.cloned.1.call-done) | copy-start | bytes 17301508
  123.3 59.9 %all-to-all-start = ((bf16[8,128,2048]{2,1,0:T(8,128)(2,1)}), bf16[8,128,2048]{2,1,0:T(8,128)(2,1)}, u32[]{:S(2)}, u32[]{:S(2)}) async-start(bf16[8,128,2048]{2,1,0:T(8,128)(2,1)} %bitcast.5), calls=%async_computation | async-start | bytes 8388608 | tf_op jit(solution)/shard_map/all_to_all | solution.py:56
  135.0 199.2 %copy-start.16 = (f32[4,704]{1,0:T(4,128)}, f32[4,704]{1,0:T(4,128)S(1)}, u32[]{:S(2)}) copy-start(f32[4,704]{1,0:T(4,128)S(1)} %broadcast_multiply_fusion) | copy-start | bytes 33796
Sparse Core Ops, SparseCore 0:
  11.1 89.4 all-gather.1
  104.6 228.3 reduce-scatter.3
